TPU v7x, 32 devices: a whole 2x2x4 slice. The times are simulated.
32 devices in a mesh: grp: 2 (over y), sp: 4 (over z), tp: 4 (over x, core).
Axes of the slice: x: 2, y: 2, z: 4, core: 2. Of those that a mesh axis runs over, the one named last changes fastest.
Arguments:
- conv_input: bfloat16 [4096, 1024], P(('grp', 'sp'), 'tp'), parts along dimension 0, may hold values from -6 to 6
- pre_gate: bfloat16 [4096, 1024], P(('grp', 'sp'), 'tp'), parts along dimension 0, may hold values from -6 to 6
- post_gate: bfloat16 [4096, 1024], P(('grp', 'sp'), 'tp'), parts along dimension 0, may hold values from -6 to 6
- conv_taps: float32 [3, 1024], replicated, may hold values from -3.5 to 3.5
- out_proj: bfloat16 [1024, 2048], replicated, may hold values from -0.1875 to 0.1875
- residual_in: bfloat16 [4096, 2048], P(('grp', 'sp', 'tp')), parts along dimension 0, may hold values from -6 to 6
- norm_gain: float32 [2048], replicated, may hold values from 0.1 to 1.9
- routes: int32 [4096, 2], P(('grp', 'sp', 'tp')), parts along dimension 0, may hold values from 0 to 7, as said below
- route_weight: float32 [4096, 2], P(('grp', 'sp', 'tp')), parts along dimension 0, may hold values from 0.1 to 1
- w_gate: bfloat16 [8, 2048, 1024], P('sp', None, 'tp'), may hold values from -0.125 to 0.125
- w_up: bfloat16 [8, 2048, 1024], P('sp', None, 'tp'), may hold values from -0.125 to 0.125
- w_down: bfloat16 [8, 1024, 2048], P('sp', 'tp'), may hold values from -0.1875 to 0.1875
Outputs:
- layer_out: bfloat16 [4096, 2048], P(('grp', 'sp', 'tp')), parts along dimension 0
There are 2 independent parts, one for each index of `grp`. A program takes and returns all parts, laid end to end along the dimension named above; an argument that names none is the same for every part. Nothing has to cross between parts.
Inputs may be any that keep to these rules, and one draw needn't show every extreme that they name: `routes`: the two numbers of a row differ and lie in the same group of 2 consecutive experts. In each aligned block of 128 rows every expert is named exactly 32 times.
All inputs are finite; a program needn't handle non-finite values.
Results may differ from a plain program's by a relative error of at most 0.0085.
Values may be sent and summed in bfloat16 or wider, within the bound.
A program may use at most 64 MiB of HBM per device.

v0:
```python
import jax
import jax.numpy as jnp
from jax import lax
from jax.sharding import PartitionSpec as P


def shifted(block, axis, distance):
    devices = range(lax.axis_size(axis))
    route = [(i - distance, i) for i in devices if i - distance in devices]
    return lax.ppermute(block, axis, route)


def on_device(
    conv_input,
    pre_gate,
    post_gate,
    conv_taps,
    out_proj,
    residual_in,
    norm_gain,
    routes,
    route_weight,
    w_gate,
    w_up,
    w_down,
):
    shards = lax.axis_size("tp")
    place = lax.axis_index("tp")
    seq_ranks = lax.axis_size("sp")
    channels = conv_input.shape[1]
    width = residual_in.shape[1]
    taps = lax.dynamic_slice_in_dim(conv_taps, place * channels, channels, 1)
    prior_input, prior_gate = shifted((conv_input[-2:], pre_gate[-2:]), "sp", 1)
    gated = jnp.concatenate(
        [
            prior_gate.astype(jnp.float32) * prior_input.astype(jnp.float32),
            pre_gate.astype(jnp.float32) * conv_input.astype(jnp.float32),
        ],
        axis=0,
    )
    conv = gated[2:] * taps[2] + gated[1:-1] * taps[1] + gated[:-2] * taps[0]
    mixed = (post_gate.astype(jnp.float32) * conv).astype(jnp.bfloat16)
    token_rows = lax.all_to_all(mixed, "tp", split_axis=0, concat_axis=1, tiled=True)
    projected = jnp.dot(token_rows, out_proj, preferred_element_type=jnp.float32)
    stream = residual_in.astype(jnp.float32) + projected
    scale = lax.rsqrt(jnp.mean(stream * stream, axis=-1, keepdims=True) + 1e-06)
    normed = (stream * scale * norm_gain).astype(jnp.bfloat16)
    block_rows = routes.shape[0]
    local_experts = w_gate.shape[0]
    experts = local_experts * seq_ranks
    capacity = 2 * block_rows // experts
    flat_routes = routes.reshape(-1)
    position = jnp.arange(flat_routes.shape[0], dtype=jnp.int32)
    earlier = (flat_routes[:, None] == flat_routes[None, :]) & (
        position[None, :] < position[:, None]
    )
    rank = jnp.sum(earlier.astype(jnp.int32), axis=1)
    slot = flat_routes * capacity + rank
    outgoing = (
        jnp.zeros((experts * capacity, width), jnp.bfloat16).at[slot].set(normed[position // 2])
    )
    outgoing = outgoing.reshape(seq_ranks, local_experts, capacity, width)
    spread = lax.all_gather(
        lax.all_to_all(outgoing, "sp", split_axis=0, concat_axis=0, tiled=True)[:, None],
        "tp",
        axis=1,
        tiled=True,
    )
    count = spread.shape[3]
    partials = []
    for expert in range(local_experts):
        rows = spread[:, :, expert].reshape(seq_ranks * shards * count, width)
        gate = jnp.dot(rows, w_gate[expert], preferred_element_type=jnp.float32)
        upper = jnp.dot(rows, w_up[expert], preferred_element_type=jnp.float32)
        hidden = (jax.nn.silu(gate) * upper).astype(jnp.bfloat16)
        part = jnp.dot(hidden, w_down[expert], preferred_element_type=jnp.float32).astype(
            jnp.bfloat16
        )
        partials.append(part.reshape(seq_ranks, shards, count, width))
    stacked = jnp.stack(partials, axis=2)
    summed = lax.psum_scatter(stacked, "tp", scatter_dimension=1, tiled=True).astype(jnp.float32)
    returned = lax.all_to_all(
        summed[:, 0].astype(jnp.bfloat16), "sp", split_axis=0, concat_axis=0, tiled=True
    )
    results = returned.reshape(experts * capacity, width)[slot]
    results = results.reshape(block_rows, 2, width).astype(jnp.float32)
    weighted = jnp.sum(route_weight[:, :, None] * results, axis=1)
    return (stream + weighted).astype(jnp.bfloat16)


def solution(mesh):
    return jax.shard_map(
        on_device,
        mesh=mesh,
        in_specs=(
            P(("grp", "sp"), "tp"),
            P(("grp", "sp"), "tp"),
            P(("grp", "sp"), "tp"),
            P(),
            P(),
            P(("grp", "sp", "tp"), None),
            P(),
            P(("grp", "sp", "tp"), None),
            P(("grp", "sp", "tp"), None),
            P("sp", None, "tp"),
            P("sp", None, "tp"),
            P("sp", "tp", None),
        ),
        out_specs=P(("grp", "sp", "tp"), None),
        check_vma=False,
    )
```

profile of v0, /device:TPU:0, one launch (start us, length us, event | category | flops | bytes accessed | tf_op | source)
XLA Modules:
  0.0 258.8 jit_solution(13987586749709506822)
XLA Ops:
  6.5 0.7 slice.46
  7.3 4.9 %collective-permute-start = (bf16[2,256]{1,0:T(2,128)(2,1)S(1)}, bf16[2,256]{1,0:T(2,128)(2,1)S(1)}, u32[]{:S(2)}, u32[]{:S(2)}) collective-permute-start(bf16[2,256]{1,0:T(2,128)(2,1)S(1)} %slice.46), channel_id=1, source_target_pairs={{0,4},{4,8},{8,12},{1,5},{5,9},{9,13},{2,6},{6,10},{10,14},{3,7},{... | collective-permute-start | bytes 3080 | tf_op jit(solution)/shard_map/ppermute | solution.py:10
  12.2 0.7 slice.47
  12.9 3.5 %collective-permute-start.1 = (bf16[2,256]{1,0:T(2,128)(2,1)S(1)}, bf16[2,256]{1,0:T(2,128)(2,1)S(1)}, u32[]{:S(2)}, u32[]{:S(2)}) collective-permute-start(bf16[2,256]{1,0:T(2,128)(2,1)S(1)} %slice.47), channel_id=1, source_target_pairs={{0,4},{4,8},{8,12},{1,5},{5,9},{9,13},{2,6},{6,10},{10,14},{3,7},{... | collective-permute-start | bytes 3080 | tf_op jit(solution)/shard_map/ppermute | solution.py:10
  16.4 1.1 convert_multiply_fusion
  17.5 0.8 copy.32
  18.3 0.7 broadcast_multiply_fusion
  19.3 0.9 fusion.46
  20.5 1.9 fusion.27
  22.4 3.4 %all-to-all-start = ((bf16[4,128,256]{2,1,0:T(8,128)(2,1)}), bf16[4,128,256]{2,1,0:T(8,128)(2,1)S(1)}, u32[]{:S(2)}, u32[]{:S(2)}) async-start(bf16[4,128,256]{2,1,0:T(8,128)(2,1)} %bitcast.3), calls=%async_computation | async-start | bytes 524288 | tf_op jit(solution)/shard_map/all_to_all | solution.py:43
  25.8 5.9 %all-to-all-done = bf16[4,128,256]{2,1,0:T(8,128)(2,1)S(1)} async-done(((bf16[4,128,256]{2,1,0:T(8,128)(2,1)}), bf16[4,128,256]{2,1,0:T(8,128)(2,1)S(1)}, u32[]{:S(2)}, u32[]{:S(2)}) %all-to-all-start) | async-done | bytes 262176 | tf_op jit(solution)/shard_map/all_to_all | solution.py:43
  31.9 3.0 %multiply_reduce_fusion.1 = (f32[128]{0:T(128)S(1)}, f32[128,2048]{1,0:T(8,128)S(1)}) fusion(bf16[128,1024]{0,1:T(8,128)(2,1)S(1)} %bitcast.62, bf16[1024,2048]{1,0:T(8,128)(2,1)} %param.16, bf16[128,2048]{1,0:T(8,128)(2,1)S(1)} %copy-done.1), kind=kOutput, calls=%fused_computation.31 | convolution fusion | flops 537919360 | bytes 6029824 | tf_op jit(solution)/shard_map/dot_general | solution.py:44
  35.1 5.7 %scatter_custom_fusion = bf16[256,2048]{1,0:T(8,128)(2,1)S(1)} fusion(s32[256]{0:T(256)S(1)} %bitcast.67, bf16[128,2048]{1,0:T(8,128)(2,1)S(1)} %multiply_convert_fusion, s32[1024]{0:T(1024)S(1)} %pad_clamp_fusion.1, bf16[]{:T(256)} %constant.35.clone.1), kind=kCustom, calls=%fused_computation.21 | custom fusion | bytes 1048578 | tf_op jit(solution)/shard_map/scatter | solution.py:60
  40.8 28.9 %all_to_all.29 = bf16[4,2,32,2048]{3,2,1,0:T(8,128)(2,1)} all-to-all(bf16[4,2,32,2048]{3,2,1,0:T(8,128)(2,1)S(1)} %bitcast.55), channel_id=1, replica_groups=mesh['grp'=2,'sp'=4,'tp'=4] {'sp'}, dimensions={0} | all-to-all | bytes 2097152 | tf_op jit(solution)/shard_map/all_to_all | solution.py:64
  70.0 32.8 %all-gather.3.cloned.1.call-done = bf16[4,8,32,2048]{3,2,1,0:T(8,128)(2,1)} async-done(((bf16[4,2,32,2048]{3,2,1,0:T(8,128)(2,1)}), bf16[4,8,32,2048]{3,2,1,0:T(8,128)(2,1)}) %all-gather.3.cloned.1.call-update) | async-done | bytes 4194320 | tf_op jit(solution)/shard_map/all_gather | solution.py:63
  102.7 2.8 %fusion.45 = (bf16[4,4,1,32,2048]{4,3,2,1,0:T(8,128)(2,1)S(1)}, bf16[4,4,1,32,2048]{4,3,2,1,0:T(8,128)(2,1)S(1)}) fusion(bf16[4,4,2,32,2048]{4,3,2,1,0:T(8,128)(2,1)} %bitcast.54), kind=kLoop, calls=%fused_computation.73 | loop fusion | bytes 8388608 | tf_op jit(solution)/shard_map/slice | solution.py:72
  105.6 1.5 fusion.10
  107.1 1.5 fusion.5
  108.6 6.0 %convolution_convert_fusion.1 = bf16[512,2048]{1,0:T(8,128)(2,1)} fusion(bf16[512,2048]{1,0:T(8,128)(2,1)} %bitcast.59, bf16[2,256,2048]{2,1,0:T(8,128)(2,1)} %param.23, bf16[2,2048,256]{2,1,0:T(8,128)(2,1)} %param.22, f32[512,256]{1,0:T(8,128)} %fusion.10), kind=kOutput, calls=%fused_computation.5 | convolution fusion | flops 1075576832 | bytes 6815744 | tf_op jit(solution)/shard_map/dot_general | solution.py:76
  114.5 5.4 %convolution_convert_fusion = bf16[512,2048]{1,0:T(8,128)(2,1)} fusion(bf16[512,2048]{1,0:T(8,128)(2,1)S(1)} %bitcast.57, bf16[2,256,2048]{2,1,0:T(8,128)(2,1)} %param.23, bf16[2,2048,256]{2,1,0:T(8,128)(2,1)} %param.22, f32[512,256]{1,0:T(8,128)} %fusion.5), kind=kOutput, calls=%fused_computation.4 | convolution fusion | flops 1075576832 | bytes 6815744 | tf_op jit(solution)/shard_map/dot_general | solution.py:76
  119.9 4.5 %pad_maximum_fusion = bf16[4,4,2,32,2048]{4,3,1,0,2:T(8,128)(2,1)} fusion(bf16[4,4,1,32,2048]{4,3,1,0,2:T(8,128)(2,1)} %bitcast.61, bf16[4,4,1,32,2048]{4,3,1,0,2:T(8,128)(2,1)} %bitcast.60), kind=kLoop, calls=%fused_computation.3 | loop fusion | flops 2097152 | bytes 8388608 | tf_op jit(solution)/shard_map/stack | solution.py:80
  124.5 0.6 copy-done.5
  125.1 0.6 dynamic-slice
  125.7 84.4 %all-reduce.3.cloned.1.call-done = bf16[4,4,2,32,2048]{4,3,1,0,2:T(8,128)(2,1)} async-done(((bf16[4,4,2,32,2048]{4,3,1,0,2:T(8,128)(2,1)}), bf16[4,4,2,32,2048]{4,3,1,0,2:T(8,128)(2,1)}) %all-reduce.3.cloned.1.call-update) | async-done | bytes 4194320
  210.1 1.9 dynamic-slice_bitcast_fusion
  212.1 1.0 copy.33
  213.1 4.6 %all-to-all-start.2 = ((bf16[4,2,32,2048]{3,2,1,0:T(8,128)(2,1)}), bf16[4,2,32,2048]{3,2,1,0:T(8,128)(2,1)S(1)}, u32[]{:S(2)}, u32[]{:S(2)}) async-start(bf16[4,2,32,2048]{3,2,1,0:T(8,128)(2,1)} %copy.33), calls=%async_computation.2 | async-start | bytes 2097152 | tf_op jit(solution)/shard_map/all_to_all | solution.py:82
  217.8 25.3 %all-to-all-done.2 = bf16[4,2,32,2048]{3,2,1,0:T(8,128)(2,1)S(1)} async-done(((bf16[4,2,32,2048]{3,2,1,0:T(8,128)(2,1)}), bf16[4,2,32,2048]{3,2,1,0:T(8,128)(2,1)S(1)}, u32[]{:S(2)}, u32[]{:S(2)}) %all-to-all-start.2) | async-done | bytes 1048608 | tf_op jit(solution)/shard_map/all_to_all | solution.py:82
  243.1 2.3 gather_fusion
  245.5 2.4 reshape.99
  247.8 3.2 %multiply_reduce_fusion = f32[128,2048]{1,0:T(8,128)S(1)} fusion(f32[128,2,2048]{2,1,0:T(2,128)S(1)} %reshape.99, f32[128,2]{1,0:T(8,128)S(1)} %copy.30), kind=kLoop, calls=%fused_computation.7 | loop fusion | flops 786432 | bytes 3146752 | tf_op jit(solution)/shard_map/reduce_sum | solution.py:87
  251.0 0.9 add_convert_fusion
  (30 shorter events, 1.4 us)
Async XLA Ops:
  6.5 25.4 %copy-start.1 = (bf16[128,2048]{1,0:T(8,128)(2,1)S(1)}, bf16[128,2048]{1,0:T(8,128)(2,1)}, u32[]{:S(2)}) copy-start(bf16[128,2048]{1,0:T(8,128)(2,1)} %param.17) | copy-start | bytes 1572868
  7.3 13.2 %collective-permute-start = (bf16[2,256]{1,0:T(2,128)(2,1)S(1)}, bf16[2,256]{1,0:T(2,128)(2,1)S(1)}, u32[]{:S(2)}, u32[]{:S(2)}) collective-permute-start(bf16[2,256]{1,0:T(2,128)(2,1)S(1)} %slice.46), channel_id=1, source_target_pairs={{0,4},{4,8},{8,12},{1,5},{5,9},{9,13},{2,6},{6,10},{10,14},{3,7},{... | collective-permute-start | bytes 3080 | tf_op jit(solution)/shard_map/ppermute | solution.py:10
  12.9 7.5 %collective-permute-start.1 = (bf16[2,256]{1,0:T(2,128)(2,1)S(1)}, bf16[2,256]{1,0:T(2,128)(2,1)S(1)}, u32[]{:S(2)}, u32[]{:S(2)}) collective-permute-start(bf16[2,256]{1,0:T(2,128)(2,1)S(1)} %slice.47), channel_id=1, source_target_pairs={{0,4},{4,8},{8,12},{1,5},{5,9},{9,13},{2,6},{6,10},{10,14},{3,7},{... | collective-permute-start | bytes 3080 | tf_op jit(solution)/shard_map/ppermute | solution.py:10
  22.4 9.4 %all-to-all-start = ((bf16[4,128,256]{2,1,0:T(8,128)(2,1)}), bf16[4,128,256]{2,1,0:T(8,128)(2,1)S(1)}, u32[]{:S(2)}, u32[]{:S(2)}) async-start(bf16[4,128,256]{2,1,0:T(8,128)(2,1)} %bitcast.3), calls=%async_computation | async-start | bytes 524288 | tf_op jit(solution)/shard_map/all_to_all | solution.py:43
  25.8 76.9 %all-gather.3.cloned.1.call-start = ((), (), s32[]{:S(2)}) async-start(), calls=%async_computation.3 | async-start | bytes 5242880 | tf_op jit(solution)/shard_map/all_gather | solution.py:63
  31.9 3.0 %copy-start.2 = (f32[2048]{0:T(1024)S(1)}, f32[2048]{0:T(1024)}, u32[]{:S(2)}) copy-start(f32[2048]{0:T(1024)} %param.18) | copy-start | bytes 24580
  69.7 140.4 %all-reduce.3.cloned.1.call-start = ((), (), s32[]{:S(2)}) async-start(), calls=%async_computation.4 | async-start | bytes 8388608
  102.7 2.9 %copy-start.4 = (bf16[2,2048,256]{2,1,0:T(8,128)(2,1)S(1)}, bf16[2,2048,256]{2,1,0:T(8,128)(2,1)}, u32[]{:S(2)}) copy-start(bf16[2,2048,256]{2,1,0:T(8,128)(2,1)} %param.21) | copy-start | bytes 6291460
  105.5 1.6 copy-start
  124.5 0.7 copy-start.5
  212.1 5.6 %copy-start.3 = (f32[128,2]{0,1:T(2,128)S(1)}, f32[128,2]{0,1:T(2,128)}, u32[]{:S(2)}) copy-start(f32[128,2]{0,1:T(2,128)} %param.20) | copy-start | bytes 3076
  213.1 30.0 %all-to-all-start.2 = ((bf16[4,2,32,2048]{3,2,1,0:T(8,128)(2,1)}), bf16[4,2,32,2048]{3,2,1,0:T(8,128)(2,1)S(1)}, u32[]{:S(2)}, u32[]{:S(2)}) async-start(bf16[4,2,32,2048]{3,2,1,0:T(8,128)(2,1)} %copy.33), calls=%async_computation.2 | async-start | bytes 2097152 | tf_op jit(solution)/shard_map/all_to_all | solution.py:82
Sparse Core Ops, SparseCore 0:
  69.8 32.8 all-gather.2
  124.6 85.4 all-reduce.2
where the time goes:
time: 259 us
  waiting for transfers between devices  148 us (57%)
  blocking collectives  28.9 us (11%)
  local copies, waits for them, and re-layouts  21.2 us (8%)
  matrix products  17.4 us (7%)
  starting transfers between devices  16.7 us (6%)
  between operations  13.6 us (5%)
  other arithmetic  12.7 us (5%)
    unnamed x3, waiting for transfers between devices  84.5 us
    all_gather x1, waiting for transfers between devices, on_device(): lax.all_gather(lax.all_to_all(outgoing, 'sp', split_axis=0, concat_axis=0...  32.8 us
    all_to_all x1, blocking collectives, on_device(): lax.all_to_all(outgoing, 'sp', split_axis=0, concat_axis=0, tiled=True)  28.9 us
    all_to_all x1, waiting for transfers between devices, on_device(): lax.all_to_all(summed[:, 0].astype(jnp.bfloat16), 'sp', split_axis=0, con...  25.3 us
    dot_general x2, matrix products, on_device(): jnp.dot(hidden, w_down[expert], preferred_element_type=jnp.float32)  11.3 us
    ppermute x2, starting transfers between devices, shifted(): return lax.ppermute(block, axis, route)  8.42 us
    all_to_all x1, waiting for transfers between devices, on_device(): lax.all_to_all(mixed, 'tp', split_axis=0, concat_axis=1, tiled=True)  5.91 us
    scatter x1, local copies, waits for them, and re-layouts, on_device(): jnp.zeros((experts * capacity, width), jnp.bfloat16).at[slot]  5.7 us
  transfers between devices with their start and end apart: 6, of which 4 were waited for; matrix products, arithmetic and copies ran while one was open for 2% of the time, Pallas kernels for 0%

commit v1 on v0

--- a/solution.py
+++ b/solution.py
@@ -60,11 +60,15 @@
         jnp.zeros((experts * capacity, width), jnp.bfloat16).at[slot].set(normed[position // 2])
     )
     outgoing = outgoing.reshape(seq_ranks, local_experts, capacity, width)
-    spread = lax.all_gather(
-        lax.all_to_all(outgoing, "sp", split_axis=0, concat_axis=0, tiled=True)[:, None],
-        "tp",
+    my_tile = lax.all_to_all(outgoing, "sp", split_axis=0, concat_axis=0, tiled=True)[:, None]
+    spread = jnp.concatenate(
+        lax.all_to_all(
+            jnp.stack(tuple((my_tile for _ in range(lax.axis_size("tp"))))),
+            axis_name="tp",
+            split_axis=0,
+            concat_axis=0,
+        ),
         axis=1,
-        tiled=True,
     )
     count = spread.shape[3]
     partials = []

time: 259 us -> 275 us (1.062)
  blocking collectives: 28.9 us -> 78.8 us
  waiting for transfers between devices: 148 us -> 114 us
    all_to_all x0 -> x1, blocking collectives: none -> 50.7 us  [on_device(): lax.all_to_all(jnp.stack(tuple((my_tile for _ in range(lax.axis_size('tp'...]
    all_gather x1 -> x0, waiting for transfers between devices: 32.8 us -> none  [on_device(): lax.all_gather(lax.all_to_all(outgoing, 'sp', split_axis=0, concat_axis=0...]
    unnamed x3 -> x2, waiting for transfers between devices: 84.5 us -> 82.6 us
  transfers between devices with their start and end apart: 6 -> 5, of which waited for: 4 -> 3; matrix products, arithmetic and copies ran while one was open for 2% -> 2% of each run, Pallas kernels for 0% -> 0%
where the time goes in v1:
time: 275 us; the launch traced here: 274 us
  waiting for transfers between devices  114 us (41%)
  blocking collectives  78.8 us (29%)
  local copies, waits for them, and re-layouts  21.6 us (8%)
  matrix products  17.4 us (6%)
  starting transfers between devices  16.5 us (6%)
  between operations  13.6 us (5%)
  other arithmetic  12.6 us (5%)
    unnamed x2, waiting for transfers between devices  82.6 us
    all_to_all x1, blocking collectives, on_device(): lax.all_to_all(jnp.stack(tuple((my_tile for _ in range(lax.axis_size('tp'...  50.7 us
    all_to_all x1, blocking collectives, on_device(): lax.all_to_all(outgoing, 'sp', split_axis=0, concat_axis=0, tiled=True)  28.1 us
    all_to_all x1, waiting for transfers between devices, on_device(): lax.all_to_all(summed[:, 0].astype(jnp.bfloat16), 'sp', split_axis=0, con...  25.3 us
    dot_general x2, matrix products, on_device(): jnp.dot(hidden, w_down[expert], preferred_element_type=jnp.float32)  11.3 us
    ppermute x2, starting transfers between devices, shifted(): return lax.ppermute(block, axis, route)  8.42 us
    all_to_all x1, waiting for transfers between devices, on_device(): lax.all_to_all(mixed, 'tp', split_axis=0, concat_axis=1, tiled=True)  5.91 us
    scatter x1, local copies, waits for them, and re-layouts, on_device(): jnp.zeros((experts * capacity, width), jnp.bfloat16).at[slot]  5.7 us
  transfers between devices with their start and end apart: 5, of which 3 were waited for; matrix products, arithmetic and copies ran while one was open for 2% of the time, Pallas kernels for 0%

profile of v1, /device:TPU:0, one launch (start us, length us, event | category | flops | bytes accessed | tf_op | source)
XLA Modules:
  0.0 274.3 jit_solution(12502963136567131496)
XLA Ops:
  6.5 0.7 slice.46
  7.3 4.9 %collective-permute-start = (bf16[2,256]{1,0:T(2,128)(2,1)S(1)}, bf16[2,256]{1,0:T(2,128)(2,1)S(1)}, u32[]{:S(2)}, u32[]{:S(2)}) collective-permute-start(bf16[2,256]{1,0:T(2,128)(2,1)S(1)} %slice.46), channel_id=1, source_target_pairs={{0,4},{4,8},{8,12},{1,5},{5,9},{9,13},{2,6},{6,10},{10,14},{3,7},{... | collective-permute-start | bytes 3080 | tf_op jit(solution)/shard_map/ppermute | solution.py:10
  12.2 0.7 slice.47
  12.9 3.5 %collective-permute-start.1 = (bf16[2,256]{1,0:T(2,128)(2,1)S(1)}, bf16[2,256]{1,0:T(2,128)(2,1)S(1)}, u32[]{:S(2)}, u32[]{:S(2)}) collective-permute-start(bf16[2,256]{1,0:T(2,128)(2,1)S(1)} %slice.47), channel_id=1, source_target_pairs={{0,4},{4,8},{8,12},{1,5},{5,9},{9,13},{2,6},{6,10},{10,14},{3,7},{... | collective-permute-start | bytes 3080 | tf_op jit(solution)/shard_map/ppermute | solution.py:10
  16.4 1.1 convert_multiply_fusion
  17.5 0.8 copy.35
  18.3 0.7 broadcast_multiply_fusion
  19.3 0.9 fusion.46
  20.5 1.9 fusion.27
  22.4 3.4 %all-to-all-start = ((bf16[4,128,256]{2,1,0:T(8,128)(2,1)}), bf16[4,128,256]{2,1,0:T(8,128)(2,1)S(1)}, u32[]{:S(2)}, u32[]{:S(2)}) async-start(bf16[4,128,256]{2,1,0:T(8,128)(2,1)} %bitcast.3), calls=%async_computation | async-start | bytes 524288 | tf_op jit(solution)/shard_map/all_to_all | solution.py:43
  25.8 5.9 %all-to-all-done = bf16[4,128,256]{2,1,0:T(8,128)(2,1)S(1)} async-done(((bf16[4,128,256]{2,1,0:T(8,128)(2,1)}), bf16[4,128,256]{2,1,0:T(8,128)(2,1)S(1)}, u32[]{:S(2)}, u32[]{:S(2)}) %all-to-all-start) | async-done | bytes 262176 | tf_op jit(solution)/shard_map/all_to_all | solution.py:43
  31.9 3.0 %multiply_reduce_fusion.1 = (f32[128]{0:T(128)S(1)}, f32[128,2048]{1,0:T(8,128)S(1)}) fusion(bf16[128,1024]{0,1:T(8,128)(2,1)S(1)} %bitcast.66, bf16[1024,2048]{1,0:T(8,128)(2,1)} %param.16, bf16[128,2048]{1,0:T(8,128)(2,1)S(1)} %copy-done.1), kind=kOutput, calls=%fused_computation.32 | convolution fusion | flops 537919360 | bytes 6029824 | tf_op jit(solution)/shard_map/dot_general | solution.py:44
  35.1 5.7 %scatter_custom_fusion = bf16[256,2048]{1,0:T(8,128)(2,1)S(1)} fusion(s32[256]{0:T(256)S(1)} %bitcast.71, bf16[128,2048]{1,0:T(8,128)(2,1)S(1)} %multiply_convert_fusion, s32[1024]{0:T(1024)S(1)} %pad_clamp_fusion.1, bf16[]{:T(256)} %constant.35.clone.1), kind=kCustom, calls=%fused_computation.22 | custom fusion | bytes 1048578 | tf_op jit(solution)/shard_map/scatter | solution.py:60
  40.8 28.1 %all_to_all.34 = bf16[4,2,32,2048]{3,2,1,0:T(8,128)(2,1)S(1)} all-to-all(bf16[4,2,32,2048]{3,2,1,0:T(8,128)(2,1)S(1)} %bitcast.59), channel_id=1, replica_groups=mesh['grp'=2,'sp'=4,'tp'=4] {'sp'}, dimensions={0} | all-to-all | bytes 2097152 | tf_op jit(solution)/shard_map/all_to_all | solution.py:63
  69.6 50.7 %all_to_all.35 = bf16[4,4,1,2,32,2048]{5,4,1,3,2,0:T(8,128)(2,1)S(1)} all-to-all(bf16[4,4,1,2,32,2048]{5,4,1,3,2,0:T(8,128)(2,1)S(1)} %stack.6), channel_id=1, replica_groups=mesh['grp'=2,'sp'=4,'tp'=4] {'tp'}, dimensions={0} | all-to-all | bytes 8388608 | tf_op jit(solution)/shard_map/all_to_all | solution.py:65
  121.3 1.7 copy-done.4
  123.0 1.5 fusion.10
  124.5 1.5 fusion.5
  126.0 6.0 %convolution_convert_fusion.1 = bf16[512,2048]{1,0:T(8,128)(2,1)} fusion(bf16[512,2048]{1,0:T(8,128)(2,1)} %bitcast.63, bf16[2,256,2048]{2,1,0:T(8,128)(2,1)} %param.23, bf16[2,2048,256]{2,1,0:T(8,128)(2,1)} %param.22, f32[512,256]{1,0:T(8,128)} %fusion.10), kind=kOutput, calls=%fused_computation.6 | convolution fusion | flops 1075576832 | bytes 6815744 | tf_op jit(solution)/shard_map/dot_general | solution.py:80
  132.0 5.3 %convolution_convert_fusion = bf16[512,2048]{1,0:T(8,128)(2,1)} fusion(bf16[512,2048]{1,0:T(8,128)(2,1)S(1)} %bitcast.61, bf16[2,256,2048]{2,1,0:T(8,128)(2,1)} %param.23, bf16[2,2048,256]{2,1,0:T(8,128)(2,1)} %param.22, f32[512,256]{1,0:T(8,128)} %fusion.5), kind=kOutput, calls=%fused_computation.5 | convolution fusion | flops 1075576832 | bytes 6815744 | tf_op jit(solution)/shard_map/dot_general | solution.py:80
  137.3 4.5 %pad_maximum_fusion = bf16[4,4,2,32,2048]{4,3,1,0,2:T(8,128)(2,1)} fusion(bf16[4,4,1,32,2048]{4,3,1,0,2:T(8,128)(2,1)} %bitcast.65, bf16[4,4,1,32,2048]{4,3,1,0,2:T(8,128)(2,1)} %bitcast.64), kind=kLoop, calls=%fused_computation.3 | loop fusion | flops 2097152 | bytes 8388608 | tf_op jit(solution)/shard_map/stack | solution.py:84
  141.9 0.6 copy-done.5
  142.5 0.6 dynamic-slice
  143.1 82.6 %all-reduce.3.cloned.1.call-done = bf16[4,4,2,32,2048]{4,3,1,0,2:T(8,128)(2,1)} async-done(((bf16[4,4,2,32,2048]{4,3,1,0,2:T(8,128)(2,1)}), bf16[4,4,2,32,2048]{4,3,1,0,2:T(8,128)(2,1)}) %all-reduce.3.cloned.1.call-update) | async-done | bytes 4194320
  225.7 1.9 dynamic-slice_bitcast_fusion
  227.6 1.0 copy.38
  228.7 4.6 %all-to-all-start.3 = ((bf16[4,2,32,2048]{3,2,1,0:T(8,128)(2,1)}), bf16[4,2,32,2048]{3,2,1,0:T(8,128)(2,1)S(1)}, u32[]{:S(2)}, u32[]{:S(2)}) async-start(bf16[4,2,32,2048]{3,2,1,0:T(8,128)(2,1)} %copy.38), calls=%async_computation.3 | async-start | bytes 2097152 | tf_op jit(solution)/shard_map/all_to_all | solution.py:86
  233.4 25.3 %all-to-all-done.3 = bf16[4,2,32,2048]{3,2,1,0:T(8,128)(2,1)S(1)} async-done(((bf16[4,2,32,2048]{3,2,1,0:T(8,128)(2,1)}), bf16[4,2,32,2048]{3,2,1,0:T(8,128)(2,1)S(1)}, u32[]{:S(2)}, u32[]{:S(2)}) %all-to-all-start.3) | async-done | bytes 1048608 | tf_op jit(solution)/shard_map/all_to_all | solution.py:86
  258.7 2.3 gather_fusion
  261.0 2.4 reshape.109
  263.4 3.2 %multiply_reduce_fusion = f32[128,2048]{1,0:T(8,128)S(1)} fusion(f32[128,2,2048]{2,1,0:T(2,128)S(1)} %reshape.109, f32[128,2]{1,0:T(8,128)S(1)} %copy.33), kind=kLoop, calls=%fused_computation.8 | loop fusion | flops 786432 | bytes 3146752 | tf_op jit(solution)/shard_map/reduce_sum | solution.py:91
  266.6 0.9 add_convert_fusion
  (31 shorter events, 2.7 us)
Async XLA Ops:
  6.5 25.4 %copy-start.1 = (bf16[128,2048]{1,0:T(8,128)(2,1)S(1)}, bf16[128,2048]{1,0:T(8,128)(2,1)}, u32[]{:S(2)}) copy-start(bf16[128,2048]{1,0:T(8,128)(2,1)} %param.17) | copy-start | bytes 1572868
  7.3 13.2 %collective-permute-start = (bf16[2,256]{1,0:T(2,128)(2,1)S(1)}, bf16[2,256]{1,0:T(2,128)(2,1)S(1)}, u32[]{:S(2)}, u32[]{:S(2)}) collective-permute-start(bf16[2,256]{1,0:T(2,128)(2,1)S(1)} %slice.46), channel_id=1, source_target_pairs={{0,4},{4,8},{8,12},{1,5},{5,9},{9,13},{2,6},{6,10},{10,14},{3,7},{... | collective-permute-start | bytes 3080 | tf_op jit(solution)/shard_map/ppermute | solution.py:10
  12.9 7.5 %collective-permute-start.1 = (bf16[2,256]{1,0:T(2,128)(2,1)S(1)}, bf16[2,256]{1,0:T(2,128)(2,1)S(1)}, u32[]{:S(2)}, u32[]{:S(2)}) collective-permute-start(bf16[2,256]{1,0:T(2,128)(2,1)S(1)} %slice.47), channel_id=1, source_target_pairs={{0,4},{4,8},{8,12},{1,5},{5,9},{9,13},{2,6},{6,10},{10,14},{3,7},{... | collective-permute-start | bytes 3080 | tf_op jit(solution)/shard_map/ppermute | solution.py:10
  22.4 9.4 %all-to-all-start = ((bf16[4,128,256]{2,1,0:T(8,128)(2,1)}), bf16[4,128,256]{2,1,0:T(8,128)(2,1)S(1)}, u32[]{:S(2)}, u32[]{:S(2)}) async-start(bf16[4,128,256]{2,1,0:T(8,128)(2,1)} %bitcast.3), calls=%async_computation | async-start | bytes 524288 | tf_op jit(solution)/shard_map/all_to_all | solution.py:43
  25.8 199.9 %all-reduce.3.cloned.1.call-start = ((), (), s32[]{:S(2)}) async-start(), calls=%async_computation.4 | async-start | bytes 8388608
  31.9 3.0 %copy-start.2 = (f32[2048]{0:T(1024)S(1)}, f32[2048]{0:T(1024)}, u32[]{:S(2)}) copy-start(f32[2048]{0:T(1024)} %param.18) | copy-start | bytes 24580
  120.9 2.1 copy-start.4
  121.3 3.2 %copy-start = (bf16[4,4,1,32,2048]{4,3,1,0,2:T(8,128)(2,1)}, bf16[4,4,1,32,2048]{4,3,1,0,2:T(8,128)(2,1)S(1)}, u32[]{:S(2)}) copy-start(bf16[4,4,1,32,2048]{4,3,1,0,2:T(8,128)(2,1)S(1)} %get-tuple-element.5) | copy-start | bytes 6291460
  141.9 0.7 copy-start.5
  227.6 5.6 %copy-start.3 = (f32[128,2]{0,1:T(2,128)S(1)}, f32[128,2]{0,1:T(2,128)}, u32[]{:S(2)}) copy-start(f32[128,2]{0,1:T(2,128)} %param.20) | copy-start | bytes 3076
  228.7 30.0 %all-to-all-start.3 = ((bf16[4,2,32,2048]{3,2,1,0:T(8,128)(2,1)}), bf16[4,2,32,2048]{3,2,1,0:T(8,128)(2,1)S(1)}, u32[]{:S(2)}, u32[]{:S(2)}) async-start(bf16[4,2,32,2048]{3,2,1,0:T(8,128)(2,1)} %copy.38), calls=%async_computation.3 | async-start | bytes 2097152 | tf_op jit(solution)/shard_map/all_to_all | solution.py:86
Sparse Core Ops, SparseCore 0:
  142.0 83.6 all-reduce.2
